TPU v7x, 32 devices: a whole 2x2x4 slice. The times are simulated.
32 devices in a mesh: dp: 4 (over y, x), kv: 4 (over z), tp: 2 (over core).
Axes of the slice: x: 2, y: 2, z: 4, core: 2. Of those that a mesh axis runs over, the one named last changes fastest.
Arguments:
- tokens: bfloat16 [32, 4096], P('dp', ('kv', 'tp')), as said below
- query_weight: bfloat16 [4096, 16, 128], P(None, 'tp', 'kv'), may hold values from -0.09375 to 0.09375
- key_weight: bfloat16 [4096, 16, 128], P(None, 'tp', 'kv'), may hold values from -0.09375 to 0.09375
- value_weight: bfloat16 [4096, 16, 256], P(None, 'tp', 'kv'), may hold values from -0.09375 to 0.09375
- gate_weight: bfloat16 [4096, 16, 256], P(None, 'tp', 'kv'), may hold values from -0.09375 to 0.09375
- decay_weight: bfloat16 [4096, 16, 128], P(None, 'tp', 'kv'), may hold values from -0.09375 to 0.09375
- decay_bias: float32 [16, 128], P('tp'), may hold values from -8 to 2
- states: float32 [32, 16, 128, 256], P(('dp', 'kv'), 'tp'), may hold values from -4 to 4
- head_gain: float32 [16, 256], P('tp'), may hold values from 0.1 to 1.9
- out_weight: bfloat16 [4096, 4096], P(None, ('kv', 'tp')), as said below
- norm1_gain: float32 [4096], P(('kv', 'tp')), may hold values from 0.1 to 1.9
- norm1_bias: float32 [4096], P(('kv', 'tp')), may hold values from -3 to 3
- up_weight: bfloat16 [4096, 16384], P(None, ('kv', 'tp')), may hold values from -0.09375 to 0.09375
- down_weight: bfloat16 [16384, 4096], P(('kv', 'tp')), as said below
- norm2_gain: float32 [4096], P(('kv', 'tp')), may hold values from 0.1 to 1.9
- norm2_bias: float32 [4096], P(('kv', 'tp')), may hold values from -3 to 3
Outputs:
- layer_out: bfloat16 [32, 4096], P('dp', ('kv', 'tp'))
- new_states: float32 [32, 16, 128, 256], P(('dp', 'kv'), 'tp')
Inputs may be any that keep to these rules, and one draw needn't show every extreme that they name: `tokens`: each block of 64 features has its own scale. `out_weight`: entries lie within 13 / sqrt(4096) of zero. `down_weight`: entries lie within 14 / sqrt(16384) of zero.
All inputs are finite; a program needn't handle non-finite values.
Results may differ from a plain program's by a relative error of at most 0.009.
Values may be sent and summed in bfloat16 or wider, within the bound.
A program may use at most 128 MiB of HBM per device.

v0:
```python
import jax
import jax.numpy as jnp
from jax import lax
from jax.sharding import PartitionSpec as P

D = 4096
KEY_DIM = 128
ALPHA = 2.0**0.5
TAU = 16.0
LN_EPS = 1e-05
RMS_EPS = 1e-06


def project_flat(inputs, weight):
    flattened = weight.reshape(weight.shape[0], -1)
    return jnp.dot(inputs, flattened, preferred_element_type=jnp.float32).astype(jnp.bfloat16)


def normalize(inputs, average, spread, row_gain, row_shift):
    return ((inputs - average) * lax.rsqrt(spread + LN_EPS) * row_gain + row_shift).astype(
        jnp.bfloat16
    )


def body(
    tokens,
    query_weight,
    key_weight,
    value_weight,
    gate_weight,
    decay_weight,
    decay_bias,
    states,
    head_gain,
    out_weight,
    norm1_gain,
    norm1_bias,
    up_weight,
    down_weight,
    norm2_gain,
    norm2_bias,
):
    whole = lax.all_gather(tokens, ("kv", "tp"), axis=1, tiled=True)
    weights_list = (query_weight, key_weight, decay_weight, value_weight, gate_weight)
    packed = jnp.concatenate([project_flat(whole, weight) for weight in weights_list], axis=1)
    arrived = lax.all_to_all(packed, "kv", split_axis=0, concat_axis=0, tiled=True)
    groups = lax.axis_size("kv")
    seq_count = whole.shape[0] // groups
    local_heads = query_weight.shape[1]
    unpacked = []
    start = 0
    for weight in weights_list:
        channels = weight.shape[2]
        width = local_heads * channels
        block = arrived[:, start : start + width].reshape(groups, seq_count, local_heads, channels)
        block = block.transpose(1, 2, 0, 3).reshape(seq_count, local_heads, groups * channels)
        unpacked.append(block.astype(jnp.float32))
        start = start + width
    query_rows = unpacked[0] * KEY_DIM ** (-0.5)
    key_rows = unpacked[1]
    decay_rows = unpacked[2]
    value_rows = unpacked[3]
    gate_rows = unpacked[4]
    retain = jnp.exp(jax.nn.log_sigmoid(decay_rows + decay_bias) / TAU)
    new_states = retain[..., None] * states + key_rows[..., :, None] * value_rows[..., None, :]
    readout = jnp.einsum("shk,shkv->shv", query_rows, new_states, precision=lax.Precision.HIGHEST)
    readout = (
        readout
        * lax.rsqrt(jnp.mean(readout * readout, axis=-1, keepdims=True) + RMS_EPS)
        * head_gain
    )
    attended = (readout * jax.nn.silu(gate_rows)).astype(jnp.bfloat16)
    seq_count, local_heads, value_width = attended.shape
    flat_width = local_heads * value_width
    collected = lax.all_gather(
        attended.reshape(1, seq_count, flat_width), ("kv", "tp"), axis=0, tiled=True
    )
    halves = lax.axis_size("tp")
    collected = collected.reshape(-1, halves, seq_count, flat_width)
    columns = out_weight.shape[1]
    out_parts = out_weight.reshape(halves, flat_width, columns)
    mixed_heads = jnp.einsum(
        "atsc,tcd->asd", collected, out_parts, preferred_element_type=jnp.float32
    ).reshape(-1, columns)
    residual_one = ALPHA * tokens.astype(jnp.float32) + mixed_heads
    offset = lax.axis_index(("kv", "tp")) * columns
    totals = lax.psum(
        (
            jnp.sum(residual_one, axis=-1, keepdims=True),
            jnp.sum(residual_one * residual_one, axis=-1, keepdims=True),
        ),
        ("kv", "tp"),
    )
    average = totals[0] / D
    spread = totals[1] / D - average * average
    normed_own = normalize(residual_one, average, spread, norm1_gain, norm1_bias)
    normed = lax.all_gather(normed_own, ("kv", "tp"), axis=1, tiled=True)
    lifted = jnp.dot(normed, up_weight, preferred_element_type=jnp.float32)
    hidden = jnp.square(jax.nn.relu(lifted)).astype(jnp.bfloat16)
    mixer_term = jnp.dot(hidden, down_weight, preferred_element_type=jnp.float32)
    mixer_all = lax.psum(mixer_term, ("kv", "tp"))
    residual_two = ALPHA * normed.astype(jnp.float32) + mixer_all
    average = jnp.sum(residual_two, axis=-1, keepdims=True) / D
    spread = jnp.sum(residual_two * residual_two, axis=-1, keepdims=True) / D - average * average
    own_rows = lax.dynamic_slice_in_dim(residual_two, offset, columns, 1)
    layer_out = normalize(own_rows, average, spread, norm2_gain, norm2_bias)
    return (layer_out, new_states)


def solution(mesh):
    placed = (
        P("dp", ("kv", "tp")),
        P(None, "tp", "kv"),
        P(None, "tp", "kv"),
        P(None, "tp", "kv"),
        P(None, "tp", "kv"),
        P(None, "tp", "kv"),
        P("tp", None),
        P(("dp", "kv"), "tp", None, None),
        P("tp", None),
        P(None, ("kv", "tp")),
        P(("kv", "tp")),
        P(("kv", "tp")),
        P(None, ("kv", "tp")),
        P(("kv", "tp"), None),
        P(("kv", "tp")),
        P(("kv", "tp")),
    )
    return jax.shard_map(
        body,
        mesh=mesh,
        in_specs=placed,
        out_specs=(P("dp", ("kv", "tp")), P(("dp", "kv"), "tp", None, None)),
        check_vma=False,
    )
```

profile of v0, /device:TPU:0, one launch (start us, length us, event | category | flops | bytes accessed | tf_op | source)
XLA Modules:
  0.0 167.2 jit_solution(12161936013294554536)
XLA Ops:
  7.2 0.0 copy-start
  7.2 0.0 all-reduce.3.cloned.1.call-start
  7.2 0.0 copy-start.4
  7.2 16.0 %all_gather.9 = bf16[8,4096]{1,0:T(8,128)(2,1)S(1)} all-gather(bf16[8,512]{1,0:T(8,128)(2,1)} %param.16), channel_id=1, replica_groups=mesh['dp'=4,'kv'=4,'tp'=2] {'kv','tp'}, dimensions={1}, use_global_device_ids=true | all-gather | bytes 73728 | tf_op jit(solution)/shard_map/all_gather | solution.py:43
  23.3 0.0 copy-done
  23.3 0.6 fusion.7
  23.9 0.0 copy-done.4
  23.9 0.0 copy-start.2
  23.9 0.7 fusion.6
  24.6 2.6 %fusion.5 = bf16[8,1792]{1,0:T(8,128)(2,1)S(1)} fusion(bf16[8,1792]{1,0:T(8,128)(2,1)S(1)} %fusion.6, bf16[8,4096]{1,0:T(8,128)(2,1)S(1)} %all_gather.9, bf16[4096,256]{0,1:T(8,128)(2,1)} %bitcast.60), kind=kOutput, calls=%fused_computation.11 | convolution fusion | flops 16779264 | bytes 2166784 | tf_op jit(solution)/shard_map/dot_general | solution.py:16
  27.2 0.0 copy-done.2
  27.2 0.0 copy-start.3
  27.2 1.2 fusion.4
  28.4 1.0 copy-done.3
  29.4 0.0 copy-start.7
  29.4 1.2 fusion.3
  30.6 10.1 %all_to_all.12 = bf16[4,2,1792]{2,1,0:T(2,128)(2,1)S(1)} all-to-all(bf16[4,2,1792]{2,1,0:T(2,128)(2,1)S(1)} %all_to_all.8), channel_id=1, replica_groups=mesh['dp'=4,'kv'=4,'tp'=2] {'kv'}, dimensions={0} | all-to-all | bytes 57344 | tf_op jit(solution)/shard_map/all_to_all | solution.py:46
  40.7 0.1 reshape.138
  40.8 0.1 reshape.134
  40.9 0.1 reshape.136
  41.0 0.1 reshape.132
  41.1 0.1 reshape.137
  41.2 0.1 reshape.133
  41.3 0.1 mul.135
  41.4 0.1 reshape.140
  41.4 0.0 copy-done.7
  41.5 1.9 %multiply_add_fusion = f32[2,8,128,256]{3,2,1,0:T(8,128)S(1)} fusion(f32[2,8,128,256]{3,2,1,0:T(8,128)} %param.23, f32[2,8,256]{2,1,0:T(8,128)S(1)} %reshape.134, f32[2,8,128]{2,1,0:T(8,128)S(1)} %reshape.133, f32[2,8,128]{2,1,0:T(8,128)S(1)} %fusion.16), kind=kLoop, calls=%fused_computation.3 | loop fusion | flops 1572864 | bytes 4227072 | tf_op jit(solution)/shard_map/add | solution.py:65
  43.4 0.0 copy-start.1
  43.4 0.0 copy-start.6
  43.4 0.0 copy-start.5
  43.4 1.3 copy-done.1
  44.7 1.1 fusion.20
  45.8 0.1 fusion.10
  45.9 0.1 reshape.139
  46.0 0.1 reshape.135
  46.1 0.0 copy-done.6
  46.1 0.1 fusion.13
  46.2 14.0 %all_gather.10 = bf16[8,2,2048]{2,1,0:T(2,128)(2,1)S(1)} all-gather(bf16[1,2,2048]{2,1,0:T(2,128)(2,1)S(1)} %reshape.129), channel_id=1, replica_groups=mesh['dp'=4,'kv'=4,'tp'=2] {'kv','tp'}, dimensions={0}, use_global_device_ids=true | all-gather | bytes 73728 | tf_op jit(solution)/shard_map/all_gather | solution.py:75
  60.3 0.0 copy-done.5
  60.3 0.0 copy-start.8
  60.3 0.0 copy-start.9
  60.3 3.0 %fusion.19 = (f32[8]{0:T(128)S(1)}, f32[8]{0:T(128)S(1)}, f32[8,512]{1,0:T(8,128)S(1)}) fusion(bf16[8,2048,2]{1,0,2:T(8,128)(2,1)S(1)} %dot_general.38, bf16[2,2048,512]{2,1,0:T(8,128)(2,1)} %bitcast.56, bf16[8,512]{1,0:T(8,128)(2,1)S(1)} %copy-done.5), kind=kOutput, calls=%fused_computation.45 | convolution fusion | flops 33578992 | bytes 4284480 | tf_op jit(solution)/shard_map/atsc,tcd->asd/dot_general | solution.py:82
  63.3 14.2 %all-reduce = (f32[8,1]{0,1:T(1,128)S(1)}, f32[8,1]{0,1:T(1,128)S(1)}) all-reduce(f32[8,1]{0,1:T(1,128)S(1)} %bitcast.69, f32[8,1]{0,1:T(1,128)S(1)} %bitcast.68), channel_id=1, replica_groups=mesh['dp'=4,'kv'=4,'tp'=2] {'kv','tp'}, use_global_device_ids=true, to_apply=%region_4.5 | all-reduce | flops 16 | bytes 128 | tf_op jit(solution)/shard_map/psum | solution.py:87
  77.6 0.0 copy-done.8
  77.6 0.0 copy-done.9
  77.6 0.1 add_convert_fusion.1
  77.7 14.0 %all_gather.11 = bf16[8,4096]{1,0:T(8,128)(2,1)S(1)} all-gather(bf16[8,512]{1,0:T(8,128)(2,1)S(1)} %add_convert_fusion.1), channel_id=1, replica_groups=mesh['dp'=4,'kv'=4,'tp'=2] {'kv','tp'}, dimensions={1}, use_global_device_ids=true | all-gather | bytes 73728 | tf_op jit(solution)/shard_map/all_gather | solution.py:97
  91.6 0.0 copy-start.10
  91.6 0.0 copy-start.11
  91.6 13.5 %fusion.8 = f32[8,4096]{1,0:T(8,128)} fusion(bf16[2048,4096]{1,0:T(8,128)(2,1)} %param.29, bf16[8,4096]{1,0:T(8,128)(2,1)S(1)} %all_gather.11, bf16[4096,2048]{1,0:T(8,128)(2,1)} %param.28), kind=kOutput, calls=%fused_computation.16 | convolution fusion | flops 268484608 | bytes 33751040 | tf_op jit(solution)/shard_map/dot_general | solution.py:100
  105.2 0.0 all-reduce.3.cloned.1.call-update
  105.2 53.4 %all-reduce.3.cloned.1.call-done = f32[8,4096]{1,0:T(8,128)} async-done(((f32[8,4096]{1,0:T(8,128)}), f32[8,4096]{1,0:T(8,128)}) %all-reduce.3.cloned.1.call-update) | async-done | bytes 131088 | tf_op jit(solution)/shard_map/psum | solution.py:101
  158.5 1.1 fusion.18
  159.6 0.0 copy-done.10
  159.6 0.0 copy-done.11
  159.6 0.7 add_convert_fusion
  (17 shorter events, 0.3 us)
Async XLA Ops:
  7.2 16.1 %copy-start = (bf16[4096,8,32]{0,2,1:T(8,128)(2,1)S(1)}, bf16[4096,8,32]{0,2,1:T(8,128)(2,1)}, u32[]{:S(2)}) copy-start(bf16[4096,8,32]{0,2,1:T(8,128)(2,1)} %param.17) | copy-start | bytes 6291460
  7.2 151.4 %all-reduce.3.cloned.1.call-start = ((), (), s32[]{:S(2)}) async-start(), calls=%async_computation.1 | async-start | bytes 262144 | tf_op jit(solution)/shard_map/psum | solution.py:101
  7.2 16.7 %copy-start.4 = (bf16[4096,8,32]{0,2,1:T(8,128)(2,1)S(1)}, bf16[4096,8,32]{0,2,1:T(8,128)(2,1)}, u32[]{:S(2)}) copy-start(bf16[4096,8,32]{0,2,1:T(8,128)(2,1)} %param.18) | copy-start | bytes 6291460
  23.9 3.2 %copy-start.2 = (bf16[4096,8,64]{0,2,1:T(8,128)(2,1)S(1)}, bf16[4096,8,64]{0,2,1:T(8,128)(2,1)}, u32[]{:S(2)}) copy-start(bf16[4096,8,64]{0,2,1:T(8,128)(2,1)} %param.19) | copy-start | bytes 12582916
  27.2 2.2 %copy-start.3 = (bf16[4096,8,64]{0,2,1:T(8,128)(2,1)S(1)}, bf16[4096,8,64]{0,2,1:T(8,128)(2,1)}, u32[]{:S(2)}) copy-start(bf16[4096,8,64]{0,2,1:T(8,128)(2,1)} %param.20) | copy-start | bytes 12582916
  29.4 12.1 %copy-start.7 = (f32[8,128]{1,0:T(8,128)S(1)}, f32[8,128]{1,0:T(8,128)}, u32[]{:S(2)}) copy-start(f32[8,128]{1,0:T(8,128)} %param.22) | copy-start | bytes 12292
  43.4 1.3 copy-start.1
  43.4 2.7 %copy-start.6 = (f32[8,256]{1,0:T(8,128)S(1)}, f32[8,256]{1,0:T(8,128)}, u32[]{:S(2)}) copy-start(f32[8,256]{1,0:T(8,128)} %param.24) | copy-start | bytes 24580
  43.4 16.9 %copy-start.5 = (bf16[8,512]{1,0:T(8,128)(2,1)S(1)}, bf16[8,512]{1,0:T(8,128)(2,1)}, u32[]{:S(2)}) copy-start(bf16[8,512]{1,0:T(8,128)(2,1)} %param.16) | copy-start | bytes 24580
  60.3 17.3 %copy-start.8 = (f32[512]{0:T(512)S(1)}, f32[512]{0:T(512)}, u32[]{:S(2)}) copy-start(f32[512]{0:T(512)} %param.27) | copy-start | bytes 6148
  60.3 17.3 %copy-start.9 = (f32[512]{0:T(512)S(1)}, f32[512]{0:T(512)}, u32[]{:S(2)}) copy-start(f32[512]{0:T(512)} %param.26) | copy-start | bytes 6148
  91.6 68.0 %copy-start.10 = (f32[512]{0:T(512)S(1)}, f32[512]{0:T(512)}, u32[]{:S(2)}) copy-start(f32[512]{0:T(512)} %param.31) | copy-start | bytes 6148
  91.6 68.0 %copy-start.11 = (f32[512]{0:T(512)S(1)}, f32[512]{0:T(512)}, u32[]{:S(2)}) copy-start(f32[512]{0:T(512)} %param.30) | copy-start | bytes 6148
Sparse Core Ops, SparseCore 0:
  105.3 53.1 all-reduce.2
where the time goes:
time: 167 us
  blocking collectives  68.3 us (41%)
  waiting for transfers between devices  53.4 us (32%)
  matrix products  23.9 us (14%)
  between operations  14.2 us (9%)
  other arithmetic  4 us (2%)
  local copies, waits for them, and re-layouts  3.36 us (2%)
    psum x1, waiting for transfers between devices, body(): mixer_all = lax.psum(mixer_term, ('kv', 'tp'))  53.4 us
    all_gather x1, blocking collectives, body(): whole = lax.all_gather(tokens, ('kv', 'tp'), axis=1, tiled=True)  16 us
    psum x1, blocking collectives, body(): lax.psum((jnp.sum(residual_one, axis=-1, keepdims=True), jnp.sum(residual...  14.2 us
    all_gather x1, blocking collectives, body(): lax.all_gather(attended.reshape(1, seq_count, flat_width), ('kv', 'tp'),...  14 us
    all_gather x1, blocking collectives, body(): normed = lax.all_gather(normed_own, ('kv', 'tp'), axis=1, tiled=True)  14 us
    dot_general x1, matrix products, body(): jnp.dot(hidden, down_weight, preferred_element_type=jnp.float32)  13.5 us
    all_to_all x1, blocking collectives, body(): lax.all_to_all(packed, 'kv', split_axis=0, concat_axis=0, tiled=True)  10.1 us
    dot_general x5, matrix products, project_flat(): jnp.dot(inputs, flattened, preferred_element_type=jnp.float32)  6.25 us
  transfers between devices with their start and end apart: 1, of which 1 were waited for; matrix products, arithmetic and copies ran while one was open for 0% of the time, Pallas kernels for 0%

commit v1 on v0

--- a/solution.py
+++ b/solution.py
@@ -85,11 +85,14 @@
     residual_one = ALPHA * tokens.astype(jnp.float32) + mixed_heads
     offset = lax.axis_index(("kv", "tp")) * columns
     totals = lax.psum(
-        (
-            jnp.sum(residual_one, axis=-1, keepdims=True),
-            jnp.sum(residual_one * residual_one, axis=-1, keepdims=True),
+        lax.psum(
+            (
+                jnp.sum(residual_one, axis=-1, keepdims=True),
+                jnp.sum(residual_one * residual_one, axis=-1, keepdims=True),
+            ),
+            "tp",
         ),
-        ("kv", "tp"),
+        "kv",
     )
     average = totals[0] / D
     spread = totals[1] / D - average * average

time: 167 us -> 165 us (0.988)
  blocking collectives: 68.3 us -> 65.6 us
    psum x1, blocking collectives: 14.2 us -> 2.48 us  [body(): lax.psum((jnp.sum(residual_one, axis=-1, keepdims=True), jnp.sum(residual...]
    psum x0 -> x1, blocking collectives: none -> 9.04 us  [body(): lax.psum(lax.psum((jnp.sum(residual_one, axis=-1, keepdims=True), jnp.sum...]
where the time goes in v1:
time: 165 us
  blocking collectives  65.6 us (40%)
  waiting for transfers between devices  54.1 us (33%)
  matrix products  23.9 us (14%)
  between operations  14.2 us (9%)
  other arithmetic  4 us (2%)
  local copies, waits for them, and re-layouts  3.36 us (2%)
    psum x1, waiting for transfers between devices, body(): mixer_all = lax.psum(mixer_term, ('kv', 'tp'))  54.1 us
    all_gather x1, blocking collectives, body(): whole = lax.all_gather(tokens, ('kv', 'tp'), axis=1, tiled=True)  16 us
    all_gather x1, blocking collectives, body(): lax.all_gather(attended.reshape(1, seq_count, flat_width), ('kv', 'tp'),...  14 us
    all_gather x1, blocking collectives, body(): normed = lax.all_gather(normed_own, ('kv', 'tp'), axis=1, tiled=True)  14 us
    dot_general x1, matrix products, body(): jnp.dot(hidden, down_weight, preferred_element_type=jnp.float32)  13.5 us
    all_to_all x1, blocking collectives, body(): lax.all_to_all(packed, 'kv', split_axis=0, concat_axis=0, tiled=True)  10.1 us
    psum x1, blocking collectives, body(): lax.psum(lax.psum((jnp.sum(residual_one, axis=-1, keepdims=True), jnp.sum...  9.04 us
    dot_general x5, matrix products, project_flat(): jnp.dot(inputs, flattened, preferred_element_type=jnp.float32)  6.25 us
  transfers between devices with their start and end apart: 1, of which 1 were waited for; matrix products, arithmetic and copies ran while one was open for 0% of the time, Pallas kernels for 0%

profile of v1, /device:TPU:0, one launch (start us, length us, event | category | flops | bytes accessed | tf_op | source)
XLA Modules:
  0.0 165.2 jit_solution(6887284719110287231)
XLA Ops:
  7.2 0.0 copy-start
  7.2 0.0 all-reduce.4.cloned.1.call-start
  7.2 0.0 copy-start.4
  7.2 16.0 %all_gather.9 = bf16[8,4096]{1,0:T(8,128)(2,1)S(1)} all-gather(bf16[8,512]{1,0:T(8,128)(2,1)} %param.16), channel_id=1, replica_groups=mesh['dp'=4,'kv'=4,'tp'=2] {'kv','tp'}, dimensions={1}, use_global_device_ids=true | all-gather | bytes 73728 | tf_op jit(solution)/shard_map/all_gather | solution.py:43
  23.3 0.0 copy-done
  23.3 0.6 fusion.7
  23.9 0.0 copy-done.4
  23.9 0.0 copy-start.2
  23.9 0.7 fusion.6
  24.6 2.6 %fusion.5 = bf16[8,1792]{1,0:T(8,128)(2,1)S(1)} fusion(bf16[8,1792]{1,0:T(8,128)(2,1)S(1)} %fusion.6, bf16[8,4096]{1,0:T(8,128)(2,1)S(1)} %all_gather.9, bf16[4096,256]{0,1:T(8,128)(2,1)} %bitcast.60), kind=kOutput, calls=%fused_computation.11 | convolution fusion | flops 16779264 | bytes 2166784 | tf_op jit(solution)/shard_map/dot_general | solution.py:16
  27.2 0.0 copy-done.2
  27.2 0.0 copy-start.3
  27.2 1.2 fusion.4
  28.4 1.0 copy-done.3
  29.4 0.0 copy-start.7
  29.4 1.2 fusion.3
  30.6 10.1 %all_to_all.12 = bf16[4,2,1792]{2,1,0:T(2,128)(2,1)S(1)} all-to-all(bf16[4,2,1792]{2,1,0:T(2,128)(2,1)S(1)} %all_to_all.8), channel_id=1, replica_groups=mesh['dp'=4,'kv'=4,'tp'=2] {'kv'}, dimensions={0} | all-to-all | bytes 57344 | tf_op jit(solution)/shard_map/all_to_all | solution.py:46
  40.7 0.1 reshape.138
  40.8 0.1 reshape.134
  40.9 0.1 reshape.136
  41.0 0.1 reshape.132
  41.1 0.1 reshape.137
  41.2 0.1 reshape.133
  41.3 0.1 mul.135
  41.4 0.1 reshape.140
  41.4 0.0 copy-done.7
  41.5 1.9 %multiply_add_fusion = f32[2,8,128,256]{3,2,1,0:T(8,128)S(1)} fusion(f32[2,8,128,256]{3,2,1,0:T(8,128)} %param.23, f32[2,8,256]{2,1,0:T(8,128)S(1)} %reshape.134, f32[2,8,128]{2,1,0:T(8,128)S(1)} %reshape.133, f32[2,8,128]{2,1,0:T(8,128)S(1)} %fusion.16), kind=kLoop, calls=%fused_computation.3 | loop fusion | flops 1572864 | bytes 4227072 | tf_op jit(solution)/shard_map/add | solution.py:65
  43.4 0.0 copy-start.1
  43.4 0.0 copy-start.6
  43.4 0.0 copy-start.5
  43.4 1.3 copy-done.1
  44.7 1.1 fusion.20
  45.8 0.1 fusion.10
  45.9 0.1 reshape.139
  46.0 0.1 reshape.135
  46.1 0.0 copy-done.6
  46.1 0.1 fusion.13
  46.2 14.0 %all_gather.10 = bf16[8,2,2048]{2,1,0:T(2,128)(2,1)S(1)} all-gather(bf16[1,2,2048]{2,1,0:T(2,128)(2,1)S(1)} %reshape.129), channel_id=1, replica_groups=mesh['dp'=4,'kv'=4,'tp'=2] {'kv','tp'}, dimensions={0}, use_global_device_ids=true | all-gather | bytes 73728 | tf_op jit(solution)/shard_map/all_gather | solution.py:75
  60.3 0.0 copy-done.5
  60.3 0.0 copy-start.8
  60.3 0.0 copy-start.9
  60.3 3.0 %fusion.19 = (f32[8]{0:T(128)S(1)}, f32[8]{0:T(128)S(1)}, f32[8,512]{1,0:T(8,128)S(1)}) fusion(bf16[8,2048,2]{1,0,2:T(8,128)(2,1)S(1)} %dot_general.38, bf16[2,2048,512]{2,1,0:T(8,128)(2,1)} %bitcast.56, bf16[8,512]{1,0:T(8,128)(2,1)S(1)} %copy-done.5), kind=kOutput, calls=%fused_computation.45 | convolution fusion | flops 33578992 | bytes 4284480 | tf_op jit(solution)/shard_map/atsc,tcd->asd/dot_general | solution.py:82
  63.3 2.5 %all-reduce.1 = (f32[8,1]{0,1:T(1,128)S(1)}, f32[8,1]{0,1:T(1,128)S(1)}) all-reduce(f32[8,1]{0,1:T(1,128)S(1)} %bitcast.69, f32[8,1]{0,1:T(1,128)S(1)} %bitcast.68), channel_id=1, replica_groups=mesh['dp'=4,'kv'=4,'tp'=2] {'tp'}, use_global_device_ids=true, to_apply=%region_5.6 | all-reduce | flops 16 | bytes 128 | tf_op jit(solution)/shard_map/psum | solution.py:88
  65.8 9.0 %all-reduce = (f32[8,1]{0,1:T(1,128)S(1)}, f32[8,1]{0,1:T(1,128)S(1)}) all-reduce(f32[8,1]{0,1:T(1,128)S(1)} %get-tuple-element.8, f32[8,1]{0,1:T(1,128)S(1)} %get-tuple-element.9), channel_id=1, replica_groups=mesh['dp'=4,'kv'=4,'tp'=2] {'kv'}, use_global_device_ids=true, to_apply=%region_6.7 | all-reduce | flops 16 | bytes 128 | tf_op jit(solution)/shard_map/psum | solution.py:87
  74.9 0.0 copy-done.8
  74.9 0.0 copy-done.9
  74.9 0.1 add_convert_fusion.1
  74.9 14.0 %all_gather.11 = bf16[8,4096]{1,0:T(8,128)(2,1)S(1)} all-gather(bf16[8,512]{1,0:T(8,128)(2,1)S(1)} %add_convert_fusion.1), channel_id=1, replica_groups=mesh['dp'=4,'kv'=4,'tp'=2] {'kv','tp'}, dimensions={1}, use_global_device_ids=true | all-gather | bytes 73728 | tf_op jit(solution)/shard_map/all_gather | solution.py:100
  88.9 0.0 copy-start.10
  88.9 0.0 copy-start.11
  88.9 13.5 %fusion.8 = f32[8,4096]{1,0:T(8,128)} fusion(bf16[2048,4096]{1,0:T(8,128)(2,1)} %param.29, bf16[8,4096]{1,0:T(8,128)(2,1)S(1)} %all_gather.11, bf16[4096,2048]{1,0:T(8,128)(2,1)} %param.28), kind=kOutput, calls=%fused_computation.16 | convolution fusion | flops 268484608 | bytes 33751040 | tf_op jit(solution)/shard_map/dot_general | solution.py:103
  102.4 0.0 all-reduce.4.cloned.1.call-update
  102.5 54.1 %all-reduce.4.cloned.1.call-done = f32[8,4096]{1,0:T(8,128)} async-done(((f32[8,4096]{1,0:T(8,128)}), f32[8,4096]{1,0:T(8,128)}) %all-reduce.4.cloned.1.call-update) | async-done | bytes 131088 | tf_op jit(solution)/shard_map/psum | solution.py:104
  156.5 1.1 fusion.18
  157.6 0.0 copy-done.10
  157.6 0.0 copy-done.11
  157.6 0.7 add_convert_fusion
  (17 shorter events, 0.3 us)
Async XLA Ops:
  7.2 16.1 %copy-start = (bf16[4096,8,32]{0,2,1:T(8,128)(2,1)S(1)}, bf16[4096,8,32]{0,2,1:T(8,128)(2,1)}, u32[]{:S(2)}) copy-start(bf16[4096,8,32]{0,2,1:T(8,128)(2,1)} %param.17) | copy-start | bytes 6291460
  7.2 149.3 %all-reduce.4.cloned.1.call-start = ((), (), s32[]{:S(2)}) async-start(), calls=%async_computation.1 | async-start | bytes 262144 | tf_op jit(solution)/shard_map/psum | solution.py:104
  7.2 16.7 %copy-start.4 = (bf16[4096,8,32]{0,2,1:T(8,128)(2,1)S(1)}, bf16[4096,8,32]{0,2,1:T(8,128)(2,1)}, u32[]{:S(2)}) copy-start(bf16[4096,8,32]{0,2,1:T(8,128)(2,1)} %param.18) | copy-start | bytes 6291460
  23.9 3.2 %copy-start.2 = (bf16[4096,8,64]{0,2,1:T(8,128)(2,1)S(1)}, bf16[4096,8,64]{0,2,1:T(8,128)(2,1)}, u32[]{:S(2)}) copy-start(bf16[4096,8,64]{0,2,1:T(8,128)(2,1)} %param.19) | copy-start | bytes 12582916
  27.2 2.2 %copy-start.3 = (bf16[4096,8,64]{0,2,1:T(8,128)(2,1)S(1)}, bf16[4096,8,64]{0,2,1:T(8,128)(2,1)}, u32[]{:S(2)}) copy-start(bf16[4096,8,64]{0,2,1:T(8,128)(2,1)} %param.20) | copy-start | bytes 12582916
  29.4 12.1 %copy-start.7 = (f32[8,128]{1,0:T(8,128)S(1)}, f32[8,128]{1,0:T(8,128)}, u32[]{:S(2)}) copy-start(f32[8,128]{1,0:T(8,128)} %param.22) | copy-start | bytes 12292
  43.4 1.3 copy-start.1
  43.4 2.7 %copy-start.6 = (f32[8,256]{1,0:T(8,128)S(1)}, f32[8,256]{1,0:T(8,128)}, u32[]{:S(2)}) copy-start(f32[8,256]{1,0:T(8,128)} %param.24) | copy-start | bytes 24580
  43.4 16.9 %copy-start.5 = (bf16[8,512]{1,0:T(8,128)(2,1)S(1)}, bf16[8,512]{1,0:T(8,128)(2,1)}, u32[]{:S(2)}) copy-start(bf16[8,512]{1,0:T(8,128)(2,1)} %param.16) | copy-start | bytes 24580
  60.3 14.6 %copy-start.8 = (f32[512]{0:T(512)S(1)}, f32[512]{0:T(512)}, u32[]{:S(2)}) copy-start(f32[512]{0:T(512)} %param.27) | copy-start | bytes 6148
  60.3 14.5 %copy-start.9 = (f32[512]{0:T(512)S(1)}, f32[512]{0:T(512)}, u32[]{:S(2)}) copy-start(f32[512]{0:T(512)} %param.26) | copy-start | bytes 6148
  88.9 68.7 %copy-start.10 = (f32[512]{0:T(512)S(1)}, f32[512]{0:T(512)}, u32[]{:S(2)}) copy-start(f32[512]{0:T(512)} %param.31) | copy-start | bytes 6148
  88.9 68.7 %copy-start.11 = (f32[512]{0:T(512)S(1)}, f32[512]{0:T(512)}, u32[]{:S(2)}) copy-start(f32[512]{0:T(512)} %param.30) | copy-start | bytes 6148
Sparse Core Ops, SparseCore 0:
  102.6 53.8 all-reduce.3
